TPU v7x, 32 devices: a whole 2x2x4 slice. The times are simulated.
32 devices in a mesh: fs: 8 (over z, y), tp: 4 (over x, core).
Axes of the slice: x: 2, y: 2, z: 4, core: 2. Of those that a mesh axis runs over, the one named last changes fastest.
Arguments:
- up_pre: bfloat16 [6144, 4096], P('fs', 'tp'), may hold values from -6 to 6
- gate_value: bfloat16 [6144, 4096], P('fs', 'tp'), may hold values from -6 to 6
- out_cotangent: bfloat16 [6144, 2048], P('fs', 'tp'), may hold values from -8 to 8
- down_weight: bfloat16 [2048, 4096], P('fs', 'tp'), may hold values from -0.09375 to 0.09375
- conv_weight: float32 [3, 4096], P(None, 'tp'), may hold values from -3.5 to 3.5
- conv_bias: float32 [4096], P('tp'), may hold values from -3 to 3
Outputs:
- up_grad: bfloat16 [6144, 4096], P('fs', 'tp')
- gate_grad: bfloat16 [6144, 4096], P('fs', 'tp')
- weight_grad: float32 [2048, 4096], P('fs', 'tp')
- tap_grad: float32 [3, 4096], P(None, 'tp')
- bias_grad: float32 [4096], P('tp')
- unit_norms: float32 [4096], P('tp')
All inputs are finite; a program needn't handle non-finite values.
Results may differ from a plain program's by a relative error of at most 0.0034.
Values may be sent and summed in bfloat16 or wider, within the bound.
A program may use at most 64 MiB of HBM per device.

v0:
```python
import functools

import jax
import jax.numpy as jnp
from jax import lax
from jax.experimental import pallas as pl
from jax.experimental.pallas import tpu as pltpu
from jax.sharding import PartitionSpec as P

MESH = pl.DeviceIdType.MESH
F32 = jnp.float32
BF16 = jnp.bfloat16


def kernel(
    fs_n, tp_n, y_n,
    up_hbm, gate_hbm, cot_ref, w_ref, cw_hbm, cb_hbm,
    ug_ref, gg_ref, wg_ref, tap_ref, bias_ref, norm_ref,
    wfull, cotf, lhs_t, hidden, act, gfac, upf, cg, pf32, pbf,
    r1, s2, r2, st, nb, halo_up, halo_cg, up_ref, gate_ref, cw_ref, cb_ref,
    local_sem, w_recv, w_send_z, w_send_y, c_recv, c_send_x, c_send_m,
    r1_recv, r1_send, r2_recv, r2_send, st_recv, st_send, nb_recv, nb_send,
    hu_sem, hc_sem,
):
    rows, cols = up_hbm.shape
    dblk = w_ref.shape[0]
    cshard = cot_ref.shape[1]
    z_n = fs_n // y_n
    x_n = tp_n // 2
    me, tp = lax.axis_index("fs"), lax.axis_index("tp")
    mz, my = me // y_n, me % y_n
    mx, mc = tp // 2, tp % 2
    mate = mx * 2 + (1 - mc)
    sends = []

    def rcopy(src, dst, ss, rs, fs_id, tp_id):
        return pltpu.make_async_remote_copy(
            src_ref=src, dst_ref=dst, send_sem=ss, recv_sem=rs,
            device_id=(fs_id, tp_id), device_id_type=MESH,
        )

    def send(*args):
        copy = rcopy(*args)
        copy.start()
        sends.append(copy)

    def wrows(owner):
        return wfull.at[pl.ds(pl.multiple_of(owner * dblk, dblk), dblk)]

    def ccols(owner):
        return cotf.at[:, pl.ds(pl.multiple_of(owner * cshard, cshard), cshard)]

    own_w = pltpu.make_async_copy(w_ref, wrows(me), local_sem.at[0])
    own_c = pltpu.make_async_copy(cot_ref, ccols(tp), local_sem.at[1])
    loads = [
        pltpu.make_async_copy(src, dst, local_sem.at[k])
        for k, (src, dst) in enumerate(
            [(up_hbm, up_ref), (gate_hbm, gate_ref), (cw_hbm, cw_ref), (cb_hbm, cb_ref)], 2
        )
    ]

    barrier = pltpu.get_barrier_semaphore()
    peers = [((me + d) % fs_n, tp) for d in range(1, fs_n)]
    peers += [(me, ((mx + d) % x_n) * 2 + mc) for d in range(1, x_n)] + [(me, mate)]
    for peer in peers:
        pl.semaphore_signal(barrier, inc=1, device_id=peer, device_id_type=MESH)
    for copy in loads:
        copy.start()
    pl.semaphore_wait(barrier, len(peers))

    @pl.when(me < fs_n - 1)
    def _():
        rcopy(up_hbm.at[pl.ds(rows - 16, 16)], halo_up, hu_sem.at[0], hu_sem.at[1], me + 1, tp).start()

    for d in range(1, x_n):
        send(cot_ref, ccols(tp), c_send_x.at[d], c_recv.at[tp], me, ((mx + d) % x_n) * 2 + mc)
    for d in range(1, z_n):
        send(w_ref, wrows(me), w_send_z.at[d], w_recv.at[me], ((mz + d) % z_n) * y_n + my, tp)
    for d in range(1, y_n):
        send(w_ref, wrows(me), w_send_y.at[d], w_recv.at[me], mz * y_n + (my + d) % y_n, tp)
    send(cot_ref, ccols(tp), c_send_m.at[0], c_recv.at[tp], me, mate)
    own_w.start()
    own_c.start()

    for copy in loads:
        copy.wait()

    @pl.when(me > 0)
    def _():
        rcopy(halo_up, halo_up, hu_sem.at[0], hu_sem.at[1], me - 1, tp).wait_recv()
        upf[0:8] = halo_up[...].astype(F32)[8:16]

    @pl.when(me == 0)
    def _():
        upf[0:8] = jnp.zeros((8, cols), F32)

    upf[8 : rows + 8] = up_ref[...].astype(F32)
    step = 64

    @pl.loop(0, cols // 128)
    def _(j):
        lanes = pl.ds(pl.multiple_of(j * 128, 128), 128)
        taps = [cw_ref[k : k + 1, lanes] for k in range(3)]
        bias = cb_ref[0:1, lanes]
        for r in range(0, rows, step):
            conv = bias + taps[0] * upf[r + 6 : r + 6 + step, lanes]
            conv = conv + taps[1] * upf[r + 7 : r + 7 + step, lanes]
            conv = conv + taps[2] * upf[r + 8 : r + 8 + step, lanes]
            sig = 1.0 / (1.0 + jnp.exp(-conv))
            a = conv * sig
            g = gate_ref[r : r + step, lanes].astype(F32)
            act[r : r + step, lanes] = a
            hidden[r : r + step, lanes] = (a * g).astype(BF16)
            gfac[r : r + step, lanes] = g * sig * (1.0 + conv * (1.0 - sig))

    def wait_cot(d, other):
        owner = ((mx + x_n - d) % x_n) * 2 + (1 - mc if other else mc)
        sem = c_send_m if other else c_send_x
        rcopy(cot_ref, ccols(owner), sem.at[d], c_recv.at[owner], me, mate if other else owner).wait_recv()
        return owner

    ywide = y_n * dblk
    tile = min(256, cols)
    own_chunks = max(z_n // x_n, 1)

    def chunk(o):
        return (mx * own_chunks + o) % z_n

    def partial_grad(o):
        zp = chunk(o)
        base = pl.multiple_of(zp * ywide, ywide)
        lhs_t[...] = cotf[:, pl.ds(base, ywide)].T

        @pl.loop(0, cols // tile)
        def _(j):
            lanes = pl.ds(pl.multiple_of(j * tile, tile), tile)
            out = jnp.dot(lhs_t[...], hidden[:, lanes], preferred_element_type=F32)
            pf32[pl.ds(base, ywide), lanes] = out
            pbf[pl.ds(base, ywide), lanes] = out.astype(BF16)

        for e in range(1, y_n):
            yp = (my + e) % y_n
            block = pl.ds(pl.multiple_of((zp * y_n + yp) * dblk, dblk), dblk)
            sem = (e - 1) * z_n + o
            send(pbf.at[block], r1.at[e - 1, o], r1_send.at[sem], r1_recv.at[sem], mz * y_n + yp, tp)

    own_c.wait()
    wait_cot(0, True)
    for o in range(own_chunks):
        partial_grad(o)
    for d in range(1, x_n):
        owner = wait_cot(d, False)
        send(ccols(owner), ccols(owner), c_send_m.at[d], c_recv.at[owner], me, mate)
    for d in range(1, x_n):
        wait_cot(d, True)
    for o in range(own_chunks, z_n):
        partial_grad(o)

    def y_sum_wait(o):
        for e in range(1, y_n):
            sem = (e - 1) * z_n + o
            rcopy(r1.at[e - 1, o], r1.at[e - 1, o], r1_send.at[sem], r1_recv.at[sem],
                  mz * y_n + (my + e) % y_n, tp).wait_recv()

    def y_sum(o, block, lanes):
        total = pf32[block, lanes]
        for e in range(1, y_n):
            total = total + r1[e - 1, o, :, lanes].astype(F32)
        return total

    def z_copy(o):
        return rcopy(s2.at[o], r2.at[mz], r2_send.at[o], r2_recv.at[mz], chunk(o) * y_n + my, tp)

    def sum_and_send(o):
        zp = chunk(o)
        block = pl.ds(pl.multiple_of((zp * y_n + my) * dblk, dblk), dblk)
        y_sum_wait(o)

        @pl.when(zp != mz)
        def _():
            @pl.loop(0, cols // 128)
            def _(j):
                lanes = pl.ds(pl.multiple_of(j * 128, 128), 128)
                s2[o, :, lanes] = y_sum(o, block, lanes).astype(BF16)

            z_copy(o).start()

    early = z_n // 2
    for o in range(early):
        sum_and_send(o)

    own_w.wait()
    for d in range(1, z_n):
        owner = ((mz + z_n - d) % z_n) * y_n + my
        rcopy(w_ref, wrows(owner), w_send_z.at[d], w_recv.at[owner], owner, tp).wait_recv()
        for e in range(1, y_n):
            send(wrows(owner), wrows(owner), w_send_y.at[d * y_n + e], w_recv.at[owner],
                 mz * y_n + (my + e) % y_n, tp)

    part_rows = 256

    def add_block(owner, first, last):
        wide = pl.multiple_of(owner * dblk, dblk)

        @pl.loop(0, cols // tile)
        def _(j):
            lanes = pl.ds(pl.multiple_of(j * tile, tile), tile)

            @pl.loop(0, rows // part_rows)
            def _(i):
                part = pl.ds(pl.multiple_of(i * part_rows, part_rows), part_rows)
                hg = jnp.dot(cotf[part, pl.ds(wide, dblk)], wfull[pl.ds(wide, dblk), lanes], preferred_element_type=F32)
                if not first:
                    hg = hg + cg[part, lanes]
                if last:
                    gg_ref[part, lanes] = (hg * act[part, lanes]).astype(BF16)
                    hg = hg * gfac[part, lanes]
                cg[part, lanes] = hg

    sum_and_send(early)
    small = dblk % 128 != 0
    if not small:
        for d in range(z_n):
            add_block(((mz + z_n - d) % z_n) * y_n + my, d == 0, False)
    for o in range(early + 1, z_n):
        sum_and_send(o)
    for d in range(z_n):
        for e in range(1, y_n):
            owner = ((mz + z_n - d) % z_n) * y_n + (my + y_n - e) % y_n
            rcopy(wrows(owner), wrows(owner), w_send_y.at[d * y_n + e], w_recv.at[owner],
                  mz * y_n + (my + e) % y_n, tp).wait_recv()
            if not small:
                add_block(owner, False, d == z_n - 1 and e == y_n - 1)
    if small:

        @pl.loop(0, cols // tile)
        def _(j):
            lanes = pl.ds(pl.multiple_of(j * tile, tile), tile)

            @pl.loop(0, rows // part_rows)
            def _(i):
                part = pl.ds(pl.multiple_of(i * part_rows, part_rows), part_rows)
                hg = jnp.dot(cotf[part, :], wfull[:, lanes], preferred_element_type=F32)
                gg_ref[part, lanes] = (hg * act[part, lanes]).astype(BF16)
                cg[part, lanes] = hg * gfac[part, lanes]

    @pl.when(me > 0)
    def _():
        rcopy(cg.at[pl.ds(0, 8)], halo_cg, hc_sem.at[0], hc_sem.at[1], me - 1, tp).start()

    @pl.loop(0, cols // 128)
    def _(j):
        lanes = pl.ds(pl.multiple_of(j * 128, 128), 128)
        sums = [jnp.zeros((8, 128), F32) for _ in range(4)]
        for r in range(0, rows, step):
            grad = cg[r : r + step, lanes]
            terms = [grad * upf[r + 6 + k : r + 6 + k + step, lanes] for k in range(3)] + [grad]
            sums = [s + jnp.sum(t.reshape(step // 8, 8, 128), axis=0) for s, t in zip(sums, terms)]
        for k in range(4):
            st[me, k : k + 1, lanes] = jnp.sum(sums[k], axis=0, keepdims=True)
        st[me, 4:8, lanes] = jnp.zeros((4, 128), F32)

    for d in range(1, fs_n):
        send(st.at[me], st.at[me], st_send.at[d], st_recv.at[me], (me + d) % fs_n, tp)

    mine = (mz + z_n - chunk(0)) % z_n
    for d in range(1, z_n):
        zp = (mz + d) % z_n
        rcopy(s2.at[0], r2.at[zp], r2_send.at[0], r2_recv.at[zp], zp * y_n + my, tp).wait_recv()
    own_block = pl.ds(pl.multiple_of(me * dblk, dblk), dblk)

    @pl.loop(0, cols // 128)
    def _(j):
        lanes = pl.ds(pl.multiple_of(j * 128, 128), 128)
        total = y_sum(mine, own_block, lanes)
        for d in range(1, z_n):
            total = total + r2[(mz + d) % z_n, :, lanes].astype(F32)
        wg_ref[:, lanes] = total
        nb[me, :, lanes] = jnp.sum(total * total, axis=0, keepdims=True)

    for d in range(1, fs_n):
        send(nb.at[me], nb.at[me], nb_send.at[d], nb_recv.at[me], (me + d) % fs_n, tp)

    @pl.when(me < fs_n - 1)
    def _():
        rcopy(halo_cg, halo_cg, hc_sem.at[0], hc_sem.at[1], me + 1, tp).wait_recv()
        cg[rows : rows + 8] = halo_cg[...]

    @pl.when(me == fs_n - 1)
    def _():
        cg[rows : rows + 8] = jnp.zeros((8, cols), F32)

    @pl.loop(0, cols // 128)
    def _(j):
        lanes = pl.ds(pl.multiple_of(j * 128, 128), 128)
        taps = [cw_ref[k : k + 1, lanes] for k in range(3)]
        for r in range(0, rows, step):
            total = taps[0] * cg[r + 2 : r + 2 + step, lanes]
            total = total + taps[1] * cg[r + 1 : r + 1 + step, lanes]
            total = total + taps[2] * cg[r : r + step, lanes]
            ug_ref[r : r + step, lanes] = total.astype(BF16)

    for d in range(1, fs_n):
        owner = (me + d) % fs_n
        rcopy(st.at[owner], st.at[owner], st_send.at[d], st_recv.at[owner], owner, tp).wait_recv()
    stats = st[0]
    for k in range(1, fs_n):
        stats = stats + st[k]
    tap_ref[...] = stats[0:3]
    bias_ref[...] = stats[3:4]
    for d in range(1, fs_n):
        owner = (me + d) % fs_n
        rcopy(nb.at[owner], nb.at[owner], nb_send.at[d], nb_recv.at[owner], owner, tp).wait_recv()
    norms = nb[0]
    for k in range(1, fs_n):
        norms = norms + nb[k]
    norm_ref[...] = norms

    for copy in sends:
        copy.wait_send()
    for o in range(z_n):

        @pl.when(chunk(o) != mz)
        def _():
            z_copy(o).wait_send()

    @pl.when(me < fs_n - 1)
    def _():
        rcopy(up_hbm.at[pl.ds(rows - 16, 16)], halo_up, hu_sem.at[0], hu_sem.at[1], me + 1, tp).wait_send()

    @pl.when(me > 0)
    def _():
        rcopy(cg.at[pl.ds(0, 8)], halo_cg, hc_sem.at[0], hc_sem.at[1], me - 1, tp).wait_send()


def per_device(fs_n, tp_n, up_pre, gate_value, out_cotangent, down_weight, conv_weight, conv_bias):
    rows, cols = up_pre.shape
    dblk = down_weight.shape[0]
    width = dblk * fs_n
    y_n = max(tp_n // 2, 2)
    z_n = fs_n // y_n
    dma = pltpu.SemaphoreType.DMA
    vmem = pl.BlockSpec(memory_space=pltpu.VMEM)
    outs = pl.pallas_call(
        functools.partial(kernel, fs_n, tp_n, y_n),
        out_shape=(
            jax.ShapeDtypeStruct((rows, cols), BF16),
            jax.ShapeDtypeStruct((rows, cols), BF16),
            jax.ShapeDtypeStruct((dblk, cols), F32),
            jax.ShapeDtypeStruct((3, cols), F32),
            jax.ShapeDtypeStruct((1, cols), F32),
            jax.ShapeDtypeStruct((1, cols), F32),
        ),
        in_specs=[pl.BlockSpec(memory_space=pltpu.HBM)] * 6,
        out_specs=[vmem] * 6,
        scratch_shapes=[
            pltpu.VMEM((width, cols), BF16),
            pltpu.VMEM((rows, width), BF16),
            pltpu.VMEM((y_n * dblk, rows), BF16),
            pltpu.VMEM((rows, cols), BF16),
            pltpu.VMEM((rows, cols), F32),
            pltpu.VMEM((rows, cols), F32),
            pltpu.VMEM((rows + 8, cols), F32),
            pltpu.VMEM((rows + 8, cols), F32),
            pltpu.VMEM((width, cols), F32),
            pltpu.VMEM((width, cols), BF16),
            pltpu.VMEM((y_n - 1, z_n, dblk, cols), BF16),
            pltpu.VMEM((z_n, dblk, cols), BF16),
            pltpu.VMEM((z_n, dblk, cols), BF16),
            pltpu.VMEM((fs_n, 8, cols), F32),
            pltpu.VMEM((fs_n, 1, cols), F32),
            pltpu.VMEM((16, cols), BF16),
            pltpu.VMEM((8, cols), F32),
            pltpu.VMEM((rows, cols), BF16),
            pltpu.VMEM((rows, cols), BF16),
            pltpu.VMEM((3, cols), F32),
            pltpu.VMEM((1, cols), F32),
            dma((6,)),
            dma((fs_n,)), dma((z_n,)), dma((z_n * y_n,)),
            dma((tp_n,)), dma((tp_n // 2,)), dma((tp_n // 2,)),
            dma(((y_n - 1) * z_n,)), dma(((y_n - 1) * z_n,)),
            dma((z_n,)), dma((z_n,)),
            dma((fs_n,)), dma((fs_n,)), dma((fs_n,)), dma((fs_n,)),
            dma((2,)), dma((2,)),
        ],
        compiler_params=pltpu.CompilerParams(
            collective_id=0, has_side_effects=True, vmem_limit_bytes=48000 * 1024
        ),
    )(
        *(
            pltpu.with_memory_space_constraint(value, pltpu.HBM)
            for value in (up_pre, gate_value, out_cotangent, down_weight, conv_weight, conv_bias[None, :])
        )
    )
    ug, gg, wg, tap, bias, norm = outs
    return ug, gg, wg, tap, bias[0], norm[0]


def solution(mesh):
    return jax.shard_map(
        functools.partial(per_device, mesh.shape["fs"], mesh.shape["tp"]),
        mesh=mesh,
        in_specs=(
            P("fs", "tp"),
            P("fs", "tp"),
            P("fs", "tp"),
            P("fs", "tp"),
            P(None, "tp"),
            P("tp"),
        ),
        out_specs=(P("fs", "tp"), P("fs", "tp"), P("fs", "tp"), P(None, "tp"), P("tp"), P("tp")),
        check_vma=False,
    )
```

profile of v0, /device:TPU:0, one launch (start us, length us, event | category | flops | bytes accessed | tf_op | source)
XLA Modules:
  0.0 117.1 jit_solution(13446904716566332275)
XLA Ops:
  0.6 111.4 %shard_map.109 = (bf16[768,1024]{1,0:T(8,128)(2,1)S(1)}, bf16[768,1024]{1,0:T(8,128)(2,1)S(1)}, f32[256,1024]{1,0:T(8,128)S(1)}, f32[3,1024]{1,0:T(4,128)S(1)}, ...) custom-call(bf16[768,1024]{1,0:T(8,128)(2,1)} %up_hbm.1, bf16[768,1024]{1,0:T(8,128)(2,1)} %gate_hbm.1, ...), custom_call_target="tpu_custom_call" | custom-call | tf_op jit(solution)/shard_map/pallas_call | solution.py:344
  112.1 1.1 copy.18
  113.2 1.1 copy.19
  114.4 1.0 copy.20
  115.3 0.6 copy.21
  115.9 0.6 copy.22
  116.5 0.6 copy.23
where the time goes:
time: 119 us; the launch traced here: 117 us
  Pallas kernels  111 us (93%)
  local copies, waits for them, and re-layouts  5.05 us (4%)
    pallas_call x1, Pallas kernels, per_device(): pl.pallas_call(functools.partial(kernel, fs_n, tp_n, y_n), out_shape=(jax...  111 us
    unnamed x6, local copies, waits for them, and re-layouts  5.05 us

commit v1 on v0

--- a/solution.py
+++ b/solution.py
@@ -333,15 +333,15 @@
         rcopy(cg.at[pl.ds(0, 8)], halo_cg, hc_sem.at[0], hc_sem.at[1], me - 1, tp).wait_send()
 
 
-def per_device(fs_n, tp_n, up_pre, gate_value, out_cotangent, down_weight, conv_weight, conv_bias):
+def general_call(fs_n, tp_n, y_n, args):
+    up_pre, _, _, down_weight, _, _ = args
     rows, cols = up_pre.shape
     dblk = down_weight.shape[0]
     width = dblk * fs_n
-    y_n = max(tp_n // 2, 2)
     z_n = fs_n // y_n
     dma = pltpu.SemaphoreType.DMA
     vmem = pl.BlockSpec(memory_space=pltpu.VMEM)
-    outs = pl.pallas_call(
+    return pl.pallas_call(
         functools.partial(kernel, fs_n, tp_n, y_n),
         out_shape=(
             jax.ShapeDtypeStruct((rows, cols), BF16),
@@ -386,12 +386,515 @@
         compiler_params=pltpu.CompilerParams(
             collective_id=0, has_side_effects=True, vmem_limit_bytes=48000 * 1024
         ),
-    )(
-        *(
-            pltpu.with_memory_space_constraint(value, pltpu.HBM)
-            for value in (up_pre, gate_value, out_cotangent, down_weight, conv_weight, conv_bias[None, :])
+    )(*args)
+
+
+def line_kernel(
+    fs_n, tp_n, y_n, n1,
+    up_hbm, gate_hbm, cot_hbm, w_hbm, cw_hbm, cb_hbm,
+    ug_ref, gg_ref, wg_ref, tap_ref, bias_ref, norm_ref,
+    wfull, cotf, lhs_t, hidden, act, gfac, upf, cg, pf32,
+    ysend, yrecv, sz1, rz1, sz2, rz2, sf, rf,
+    st, nb, halo_up, halo_cg, up_ref, gate_ref, cw_ref, cb_ref,
+    local_sem, ag_send, ag_recv, yw_send, yw_recv, yp_sem, c_send, c_recv, ry_send, ry_recv,
+    rs_send, rs_recv, f_sem, st_recv, st_send, nb_recv, nb_send, hu_sem, hc_sem,
+):
+    rows, cols = up_hbm.shape
+    dblk = w_hbm.shape[0]
+    cshard = cot_hbm.shape[1]
+    ywide = y_n * dblk
+    z_n = fs_n // y_n
+    n2 = cols - n1
+    me, tp = lax.axis_index("fs"), lax.axis_index("tp")
+    mz, my = me // y_n, me % y_n
+    mx, mc = tp // 2, tp % 2
+    mate = mx * 2 + (1 - mc)
+    mirror = (1 - mx) * 2 + mc
+    across = (1 - mx) * 2 + (1 - mc)
+    ynb = mz * y_n + (1 - my)
+    sign = (1, -1)
+    avail = (mz, z_n - 1 - mz)
+    has_next = (mz < z_n - 1, mz > 0)
+    has_prev = (mz > 0, mz < z_n - 1)
+    nxt = [((mz + z_n + s) % z_n) * y_n + my for s in sign]
+    sends = []
+
+    def rcopy(src, dst, ss, rs, fs_id, tp_id):
+        return pltpu.make_async_remote_copy(
+            src_ref=src, dst_ref=dst, send_sem=ss, recv_sem=rs,
+            device_id=(fs_id, tp_id), device_id_type=MESH,
         )
+
+    def start(make, pred=None, inside=None):
+        if pred is None:
+            make().start()
+        else:
+            @pl.when(pred if inside is None else inside)
+            def _():
+                make().start()
+        sends.append((pred, make))
+
+    def drows(zp, y):
+        return pl.ds(pl.multiple_of((zp * y_n + y) * dblk, dblk), dblk)
+
+    def ccols(owner):
+        return cotf.at[:, pl.ds(pl.multiple_of(owner * cshard, cshard), cshard)]
+
+    part1, part2 = pl.ds(0, n1), pl.ds(n1, n2)
+
+    def ag_copy(d, slot, part, zp):
+        ref = wfull.at[drows(zp, 1 - my if part == 2 else my), part1 if part == 1 else part2]
+        src = ref
+        if slot == 0 and part < 2:
+            src = w_hbm.at[:, part1 if part == 1 else part2]
+        i = (d * z_n + slot) * 3 + part
+        return rcopy(src, ref, ag_send.at[i], ag_recv.at[i], nxt[d], tp)
+
+    def yw_copy(zp, own=False):
+        ref = wfull.at[drows(zp, my), part1]
+        return rcopy(w_hbm.at[:, part1] if own else ref, ref, yw_send.at[zp], yw_recv.at[zp], ynb, tp)
+
+    def yw_wait(zp):
+        ref = wfull.at[drows(zp, 1 - my), part1]
+        rcopy(ref, ref, yw_send.at[zp], yw_recv.at[zp], ynb, tp).wait_recv()
+
+    def rs_copy(d, slot, part, t):
+        i = (d * z_n + slot) * 2 + part
+        src, dst = (sz2.at[t], rz2.at[d, t]) if part == 0 else (sz1.at[t], rz1.at[d, t])
+        return rcopy(src, dst, rs_send.at[i], rs_recv.at[i], nxt[d], tp)
+
+    def ry_copy(t):
+        return rcopy(ysend.at[t], yrecv.at[t], ry_send.at[t], ry_recv.at[t], ynb, tp)
+
+    own_w = pltpu.make_async_copy(w_hbm, wfull.at[drows(mz, my)], local_sem.at[0])
+    own_c = pltpu.make_async_copy(cot_hbm, ccols(tp), local_sem.at[1])
+    loads = [
+        pltpu.make_async_copy(src, dst, local_sem.at[k])
+        for k, (src, dst) in enumerate(
+            [(up_hbm, up_ref), (gate_hbm, gate_ref), (cw_hbm, cw_ref), (cb_hbm, cb_ref)], 2
+        )
+    ]
+
+    barrier = pltpu.get_barrier_semaphore()
+    peers = [((me + d) % fs_n, tp) for d in range(1, fs_n)] + [(me, mirror), (me, mate)]
+    for peer in peers:
+        pl.semaphore_signal(barrier, inc=1, device_id=peer, device_id_type=MESH)
+    for copy in loads:
+        copy.start()
+    own_c.start()
+    own_w.start()
+    pl.semaphore_wait(barrier, len(peers))
+
+    start(
+        lambda: rcopy(up_hbm.at[pl.ds(rows - 16, 16)], halo_up, hu_sem.at[0], hu_sem.at[1], (me + 1) % fs_n, tp),
+        me < fs_n - 1,
     )
+    yp_copy = lambda: rcopy(
+        w_hbm.at[:, part2], wfull.at[drows(mz, my), part2], yp_sem.at[0], yp_sem.at[1], ynb, tp
+    )
+    start(yp_copy)
+    for part in (0, 1):
+        for d in (0, 1):
+            start(functools.partial(ag_copy, d, 0, part, mz), has_next[d])
+    start(functools.partial(yw_copy, mz, True))
+    start(lambda: rcopy(cot_hbm, ccols(tp), c_send.at[0], c_recv.at[tp], me, mirror))
+    start(lambda: rcopy(cot_hbm, ccols(tp), c_send.at[1], c_recv.at[tp], me, mate))
+
+    for copy in loads:
+        copy.wait()
+
+    @pl.when(me > 0)
+    def _():
+        rcopy(halo_up, halo_up, hu_sem.at[0], hu_sem.at[1], (me + fs_n - 1) % fs_n, tp).wait_recv()
+        upf[0:8] = halo_up[...].astype(F32)[8:16]
+
+    @pl.when(me == 0)
+    def _():
+        upf[0:8] = jnp.zeros((8, cols), F32)
+
+    upf[8 : rows + 8] = up_ref[...].astype(F32)
+    step = 64
+
+    @pl.loop(0, cols // 128)
+    def _(j):
+        lanes = pl.ds(pl.multiple_of(j * 128, 128), 128)
+        taps = [cw_ref[k : k + 1, lanes] for k in range(3)]
+        bias = cb_ref[0:1, lanes]
+        for r in range(0, rows, step):
+            conv = bias + taps[0] * upf[r + 6 : r + 6 + step, lanes]
+            conv = conv + taps[1] * upf[r + 7 : r + 7 + step, lanes]
+            conv = conv + taps[2] * upf[r + 8 : r + 8 + step, lanes]
+            sig = 1.0 / (1.0 + jnp.exp(-conv))
+            a = conv * sig
+            g = gate_ref[r : r + step, lanes].astype(F32)
+            act[r : r + step, lanes] = a
+            hidden[r : r + step, lanes] = (a * g).astype(BF16)
+            gfac[r : r + step, lanes] = g * sig * (1.0 + conv * (1.0 - sig))
+
+    rcopy(
+        w_hbm.at[:, part2], wfull.at[drows(mz, 1 - my), part2], yp_sem.at[0], yp_sem.at[1], ynb, tp
+    ).wait_recv()
+    for d in (0, 1):
+        start(functools.partial(ag_copy, d, 0, 2, mz), has_next[d])
+
+    tile = min(256, cols)
+
+    def wg_part(t):
+        base = pl.multiple_of(t * ywide, ywide)
+        lhs_t[...] = cotf[:, pl.ds(base, ywide)].T
+
+        @pl.loop(0, cols // tile)
+        def _(j):
+            lanes = pl.ds(pl.multiple_of(j * tile, tile), tile)
+            pf32[pl.ds(base, ywide), lanes] = jnp.dot(lhs_t[...], hidden[:, lanes], preferred_element_type=F32)
+
+        @pl.loop(0, n1 // 128)
+        def _(j):
+            lanes = pl.ds(pl.multiple_of(j * 128, 128), 128)
+            ysend[t, :, lanes] = pf32[drows(t, 1 - my), lanes].astype(BF16)
+
+    def wg_half(half):
+        low = half * (z_n // 2)
+        first = jnp.where(half == 0, jnp.where(mz == 0, 1, 0), jnp.where(mz == z_n - 1, 0, 1))
+        wg_part(low + first)
+        wg_part(low + 1 - first)
+
+    def ry_start(delta, half=None):
+        for s in sign if delta else (1,):
+            t = mz + s * delta
+            pred = (t >= 0) & (t < z_n)
+            t = (t + z_n) % z_n
+            if half is not None:
+                pred = pred & (t // (z_n // 2) == half)
+            start(functools.partial(ry_copy, t), pred)
+
+    own_c.wait()
+    rcopy(cot_hbm, ccols(mate), c_send.at[1], c_recv.at[mate], me, mate).wait_recv()
+    wg_half(mx)
+    ry_start(z_n - 1, mx)
+
+    def ag_step(k):
+        for d in (0, 1):
+            zp = (mz + z_n - sign[d] * (1 + k)) % z_n
+            is_ag = k < avail[d]
+            fwd = is_ag & has_next[d]
+
+            @pl.when(is_ag)
+            def _():
+                for part in (0, 1, 2):
+                    ag_copy(d, k, part, zp).wait_recv()
+                    if k + 1 < z_n - 1:
+                        @pl.when(has_next[d])
+                        def _():
+                            ag_copy(d, k + 1, part, zp).start()
+                    if part == 1:
+                        yw_copy(zp).start()
+
+            for part in (0, 1, 2):
+                if k + 1 < z_n - 1:
+                    sends.append((fwd, functools.partial(ag_copy, d, k + 1, part, zp)))
+            sends.append((is_ag, functools.partial(yw_copy, zp)))
+
+    def rs_step(k):
+        for d in (0, 1):
+            t = (mz + z_n - sign[d] * (1 + k)) % z_n
+            pred = k >= avail[d]
+
+            def run(arrived, d=d, t=t):
+                if arrived:
+                    rs_copy(d, k, 0, t).wait_recv()
+
+                @pl.loop(0, n2 // 128)
+                def _(j):
+                    far = pl.ds(pl.multiple_of(n1 + j * 128, 128), 128)
+                    near = pl.ds(pl.multiple_of(j * 128, 128), 128)
+                    total = pf32[pl.ds(pl.multiple_of(t * ywide, ywide), ywide), far]
+                    if arrived:
+                        total = total + rz2[d, t, :, near].astype(F32)
+                    sz2[t, :, near] = total.astype(BF16)
+
+                rs_copy(d, k + 1, 0, t).start()
+                ry_copy(t).wait_recv()
+                if arrived:
+                    rs_copy(d, k, 1, t).wait_recv()
+
+                @pl.loop(0, n1 // 128)
+                def _(j):
+                    lanes = pl.ds(pl.multiple_of(j * 128, 128), 128)
+                    total = pf32[drows(t, my), lanes] + yrecv[t, :, lanes].astype(F32)
+                    if arrived:
+                        total = total + rz1[d, t, :, lanes].astype(F32)
+                    sz1[t, :, lanes] = total.astype(BF16)
+
+                rs_copy(d, k + 1, 1, t).start()
+
+            if k > 0:
+                pl.when(pred & has_prev[d])(functools.partial(run, True))
+            pl.when(pred & jnp.logical_not(has_prev[d]))(functools.partial(run, False))
+            for part in (0, 1):
+                sends.append((pred, functools.partial(rs_copy, d, k + 1, part, t)))
+
+    part_rows = rows // 2 if rows % 32 == 0 else rows
+
+    def hg_add(zp, first):
+        base = pl.ds(pl.multiple_of(zp * ywide, ywide), ywide)
+
+        @pl.loop(0, cols // tile)
+        def _(j):
+            lanes = pl.ds(pl.multiple_of(j * tile, tile), tile)
+
+            @pl.loop(0, rows // part_rows)
+            def _(i):
+                part = pl.ds(pl.multiple_of(i * part_rows, part_rows), part_rows)
+                hg = jnp.dot(cotf[part, base], wfull[base, lanes], preferred_element_type=F32)
+                if not first:
+                    hg = hg + cg[part, lanes]
+                cg[part, lanes] = hg
+
+    def hg_far(delta):
+        for s in sign:
+            zp = mz + s * delta
+
+            @pl.when((zp >= 0) & (zp < z_n))
+            def _():
+                near = (zp + z_n) % z_n
+                yw_wait(near)
+                hg_add(near, False)
+
+    ag_step(0)
+    rcopy(cot_hbm, ccols(mirror), c_send.at[0], c_recv.at[mirror], me, mirror).wait_recv()
+    start(lambda: rcopy(ccols(mirror), ccols(mirror), c_send.at[2], c_recv.at[mirror], me, mate))
+    rcopy(cot_hbm, ccols(across), c_send.at[2], c_recv.at[across], me, mate).wait_recv()
+    wg_half(1 - mx)
+    ry_start(z_n - 1, 1 - mx)
+    for delta in range(z_n - 2, 1, -1):
+        ry_start(delta)
+    rs_step(0)
+    own_w.wait()
+    yw_wait(mz)
+    hg_add(mz, True)
+    for k in range(1, z_n - 1):
+        ag_step(k)
+        if k == 1:
+            ry_start(1)
+        if k == z_n - 2:
+            ry_start(0)
+        rs_step(k)
+        hg_far(k)
+    hg_far(z_n - 1)
+
+    @pl.loop(0, cols // 128)
+    def _(j):
+        lanes = pl.ds(pl.multiple_of(j * 128, 128), 128)
+        for r in range(0, rows, step):
+            part = slice(r, r + step)
+            hg = cg[part, lanes]
+            gg_ref[part, lanes] = (hg * act[part, lanes]).astype(BF16)
+            cg[part, lanes] = hg * gfac[part, lanes]
+
+    start(
+        lambda: rcopy(cg.at[pl.ds(0, 8)], halo_cg, hc_sem.at[0], hc_sem.at[1], (me + fs_n - 1) % fs_n, tp),
+        me > 0,
+    )
+
+    @pl.loop(0, cols // 128)
+    def _(j):
+        lanes = pl.ds(pl.multiple_of(j * 128, 128), 128)
+        sums = [jnp.zeros((8, 128), F32) for _ in range(4)]
+        for r in range(0, rows, step):
+            grad = cg[r : r + step, lanes]
+            terms = [grad * upf[r + 6 + k : r + 6 + k + step, lanes] for k in range(3)] + [grad]
+            sums = [s + jnp.sum(t.reshape(step // 8, 8, 128), axis=0) for s, t in zip(sums, terms)]
+        for k in range(4):
+            st[me, k : k + 1, lanes] = jnp.sum(sums[k], axis=0, keepdims=True)
+
+    for d in range(1, fs_n):
+        start(
+            lambda d=d: rcopy(st.at[me], st.at[me], st_send.at[d], st_recv.at[me], (me + d) % fs_n, tp)
+        )
+
+    last = z_n - 1
+    for d in (0, 1):
+
+        @pl.when(has_prev[d])
+        def _():
+            rs_copy(d, last, 0, mz).wait_recv()
+
+            @pl.loop(0, n2 // 128)
+            def _(j):
+                far = pl.ds(pl.multiple_of(n1 + j * 128, 128), 128)
+                near = pl.ds(pl.multiple_of(j * 128, 128), 128)
+                block = pl.ds(pl.multiple_of(mz * ywide, ywide), ywide)
+                pf32[block, far] = pf32[block, far] + rz2[d, mz, :, near].astype(F32)
+
+    @pl.loop(0, n2 // 128)
+    def _(j):
+        far = pl.ds(pl.multiple_of(n1 + j * 128, 128), 128)
+        near = pl.ds(pl.multiple_of(j * 128, 128), 128)
+        sf[:, near] = pf32[drows(mz, 1 - my), far].astype(BF16)
+
+    f_copy = lambda: rcopy(sf, rf, f_sem.at[0], f_sem.at[1], ynb, tp)
+    start(f_copy)
+
+    @pl.when(me < fs_n - 1)
+    def _():
+        rcopy(halo_cg, halo_cg, hc_sem.at[0], hc_sem.at[1], (me + 1) % fs_n, tp).wait_recv()
+        cg[rows : rows + 8] = halo_cg[...]
+
+    @pl.when(me == fs_n - 1)
+    def _():
+        cg[rows : rows + 8] = jnp.zeros((8, cols), F32)
+
+    @pl.loop(0, cols // 128)
+    def _(j):
+        lanes = pl.ds(pl.multiple_of(j * 128, 128), 128)
+        taps = [cw_ref[k : k + 1, lanes] for k in range(3)]
+        for r in range(0, rows, step):
+            total = taps[0] * cg[r + 2 : r + 2 + step, lanes]
+            total = total + taps[1] * cg[r + 1 : r + 1 + step, lanes]
+            total = total + taps[2] * cg[r : r + step, lanes]
+            ug_ref[r : r + step, lanes] = total.astype(BF16)
+
+    own_block = drows(mz, my)
+    ry_copy(mz).wait_recv()
+
+    @pl.loop(0, n1 // 128)
+    def _(j):
+        lanes = pl.ds(pl.multiple_of(j * 128, 128), 128)
+        wg_ref[:, lanes] = pf32[own_block, lanes] + yrecv[mz, :, lanes].astype(F32)
+
+    for d in (0, 1):
+
+        @pl.when(has_prev[d])
+        def _():
+            rs_copy(d, last, 1, mz).wait_recv()
+
+            @pl.loop(0, n1 // 128)
+            def _(j):
+                lanes = pl.ds(pl.multiple_of(j * 128, 128), 128)
+                wg_ref[:, lanes] = wg_ref[:, lanes] + rz1[d, mz, :, lanes].astype(F32)
+
+    f_copy().wait_recv()
+
+    @pl.loop(0, n2 // 128)
+    def _(j):
+        far = pl.ds(pl.multiple_of(n1 + j * 128, 128), 128)
+        near = pl.ds(pl.multiple_of(j * 128, 128), 128)
+        wg_ref[:, far] = pf32[own_block, far] + rf[:, near].astype(F32)
+
+    @pl.loop(0, cols // 128)
+    def _(j):
+        lanes = pl.ds(pl.multiple_of(j * 128, 128), 128)
+        total = wg_ref[:, lanes]
+        nb[me, :, lanes] = jnp.sum(total * total, axis=0, keepdims=True)
+
+    for d in range(1, fs_n):
+        start(
+            lambda d=d: rcopy(nb.at[me], nb.at[me], nb_send.at[d], nb_recv.at[me], (me + d) % fs_n, tp)
+        )
+
+    for d in range(1, fs_n):
+        owner = (me + d) % fs_n
+        rcopy(st.at[owner], st.at[owner], st_send.at[d], st_recv.at[owner], owner, tp).wait_recv()
+    stats = st[0]
+    for k in range(1, fs_n):
+        stats = stats + st[k]
+    tap_ref[...] = stats[0:3]
+    bias_ref[...] = stats[3:4]
+
+    for pred, make in sends:
+        if pred is None:
+            make().wait_send()
+        else:
+            @pl.when(pred)
+            def _():
+                make().wait_send()
+
+    for d in range(1, fs_n):
+        owner = (me + d) % fs_n
+        rcopy(nb.at[owner], nb.at[owner], nb_send.at[d], nb_recv.at[owner], owner, tp).wait_recv()
+    norms = nb[0]
+    for k in range(1, fs_n):
+        norms = norms + nb[k]
+    norm_ref[...] = norms
+
+
+def line_call(fs_n, tp_n, y_n, args):
+    up_pre, _, _, down_weight, _, _ = args
+    rows, cols = up_pre.shape
+    dblk = down_weight.shape[0]
+    width = dblk * fs_n
+    ywide = y_n * dblk
+    z_n = fs_n // y_n
+    n2 = max(cols * 3 // 8 // 128, 1) * 128
+    n1 = cols - n2
+    dma = pltpu.SemaphoreType.DMA
+    vmem = pl.BlockSpec(memory_space=pltpu.VMEM)
+    return pl.pallas_call(
+        functools.partial(line_kernel, fs_n, tp_n, y_n, n1),
+        out_shape=(
+            jax.ShapeDtypeStruct((rows, cols), BF16),
+            jax.ShapeDtypeStruct((rows, cols), BF16),
+            jax.ShapeDtypeStruct((dblk, cols), F32),
+            jax.ShapeDtypeStruct((3, cols), F32),
+            jax.ShapeDtypeStruct((1, cols), F32),
+            jax.ShapeDtypeStruct((1, cols), F32),
+        ),
+        in_specs=[pl.BlockSpec(memory_space=pltpu.HBM)] * 6,
+        out_specs=[vmem] * 6,
+        scratch_shapes=[
+            pltpu.VMEM((width, cols), BF16),
+            pltpu.VMEM((rows, width), BF16),
+            pltpu.VMEM((ywide, rows), BF16),
+            pltpu.VMEM((rows, cols), BF16),
+            pltpu.VMEM((rows, cols), F32),
+            pltpu.VMEM((rows, cols), F32),
+            pltpu.VMEM((rows + 8, cols), F32),
+            pltpu.VMEM((rows + 8, cols), F32),
+            pltpu.VMEM((width, cols), F32),
+            pltpu.VMEM((z_n, dblk, n1), BF16),
+            pltpu.VMEM((z_n, dblk, n1), BF16),
+            pltpu.VMEM((z_n, dblk, n1), BF16),
+            pltpu.VMEM((2, z_n, dblk, n1), BF16),
+            pltpu.VMEM((z_n, ywide, n2), BF16),
+            pltpu.VMEM((2, z_n, ywide, n2), BF16),
+            pltpu.VMEM((dblk, n2), BF16),
+            pltpu.VMEM((dblk, n2), BF16),
+            pltpu.VMEM((fs_n, 4, cols), F32),
+            pltpu.VMEM((fs_n, 1, cols), F32),
+            pltpu.VMEM((16, cols), BF16),
+            pltpu.VMEM((8, cols), F32),
+            pltpu.VMEM((rows, cols), BF16),
+            pltpu.VMEM((rows, cols), BF16),
+            pltpu.VMEM((3, cols), F32),
+            pltpu.VMEM((1, cols), F32),
+            dma((6,)),
+            dma((6 * z_n,)), dma((6 * z_n,)), dma((z_n,)), dma((z_n,)), dma((2,)),
+            dma((3,)), dma((tp_n,)), dma((z_n,)), dma((z_n,)),
+            dma((4 * z_n,)), dma((4 * z_n,)), dma((2,)),
+            dma((fs_n,)), dma((fs_n,)), dma((fs_n,)), dma((fs_n,)),
+            dma((2,)), dma((2,)),
+        ],
+        compiler_params=pltpu.CompilerParams(
+            collective_id=0, has_side_effects=True, vmem_limit_bytes=56000 * 1024
+        ),
+    )(*args)
+
+
+def per_device(fs_n, tp_n, up_pre, gate_value, out_cotangent, down_weight, conv_weight, conv_bias):
+    rows, cols = up_pre.shape
+    dblk = down_weight.shape[0]
+    width = dblk * fs_n
+    y_n = max(tp_n // 2, 2)
+    z_n = fs_n // y_n
+    args = tuple(
+        pltpu.with_memory_space_constraint(value, pltpu.HBM)
+        for value in (up_pre, gate_value, out_cotangent, down_weight, conv_weight, conv_bias[None, :])
+    )
+    if tp_n == 4 and z_n == tp_n and rows % 64 == 0 and cols % 256 == 0 and dblk % 128 == 0:
+        outs = line_call(fs_n, tp_n, y_n, args)
+    else:
+        outs = general_call(fs_n, tp_n, y_n, args)
     ug, gg, wg, tap, bias, norm = outs
     return ug, gg, wg, tap, bias[0], norm[0]
 

time: 119 us -> 98.8 us (0.83); the launches traced: 117 us -> 98.4 us
  Pallas kernels: 111 us -> 90.4 us
  local copies, waits for them, and re-layouts: 5.05 us -> 7.36 us
    pallas_call x1, Pallas kernels: 111 us -> 90.4 us  [line_call(): pl.pallas_call(functools.partial(line_kernel, fs_n, tp_n, y_n, n1), out_s...]
    unnamed x6 -> x16, local copies, waits for them, and re-layouts: 5.05 us -> 7.36 us
where the time goes in v1:
time: 98.8 us; the launch traced here: 98.4 us
  Pallas kernels  90.4 us (91%)
  local copies, waits for them, and re-layouts  7.36 us (7%)
    pallas_call x1, Pallas kernels, line_call(): pl.pallas_call(functools.partial(line_kernel, fs_n, tp_n, y_n, n1), out_s...  90.4 us
    unnamed x16, local copies, waits for them, and re-layouts  7.36 us

profile of v1, /device:TPU:0, one launch (start us, length us, event | category | flops | bytes accessed | tf_op | source)
XLA Modules:
  0.0 98.4 jit_solution(16476886206410375484)
XLA Ops:
  0.6 90.4 %shard_map.109 = (bf16[768,1024]{1,0:T(8,128)(2,1)}, bf16[768,1024]{1,0:T(8,128)(2,1)}, f32[256,1024]{1,0:T(8,128)}, f32[3,1024]{1,0:T(4,128)}, f32[1,1024]{1,0:T(1,128)}, /*index=5*/f32[1,1024]{1,0:T(1,128)}) custom-call(bf16[768,1024]{1,0:T(8,128)(2,1)} %up_hbm.1, bf16[768,1024]{1,0:T(8,128)(2,1)} %gate_hbm.1, bf16[768,512]{1,0:T(8,128)(2,1)} %cot_hbm.1, ...), custom_call_target="tpu_custom_call" | custom-call | tf_op jit(solution)/shard_map/pallas_call | solution.py:833
  91.0 0.0 copy-start
  91.0 2.8 %copy.18 = bf16[768,1024]{1,0:T(8,128)(2,1)} copy(bf16[768,1024]{1,0:T(8,128)(2,1)} %get-tuple-element.24) | data formatting | bytes 3145728
  93.8 0.0 copy-done
  93.8 0.0 copy-start.1
  93.8 1.1 %copy.19 = bf16[768,1024]{1,0:T(8,128)(2,1)} copy(bf16[768,1024]{1,0:T(8,128)(2,1)S(1)} %copy-done) | data formatting | bytes 3145728
  94.9 0.6 copy-done.1
  95.6 0.0 copy-start.2
  95.6 0.0 copy-start.4
  95.6 0.0 copy-start.3
  95.6 1.0 copy.20
  96.6 0.0 copy-done.2
  96.6 0.6 copy.21
  97.2 0.0 copy-done.4
  97.2 0.6 copy.22
  97.8 0.0 copy-done.3
  97.8 0.6 copy.23
Async XLA Ops:
  91.0 2.8 %copy-start = (bf16[768,1024]{1,0:T(8,128)(2,1)S(1)}, bf16[768,1024]{1,0:T(8,128)(2,1)}, u32[]{:S(2)}) copy-start(bf16[768,1024]{1,0:T(8,128)(2,1)} %get-tuple-element.25) | copy-start | bytes 4718596
  93.8 1.8 %copy-start.1 = (f32[256,1024]{1,0:T(8,128)S(1)}, f32[256,1024]{1,0:T(8,128)}, u32[]{:S(2)}) copy-start(f32[256,1024]{1,0:T(8,128)} %get-tuple-element.26) | copy-start | bytes 3145732
  95.6 1.0 copy-start.2
  95.6 1.6 %copy-start.4 = (f32[1,1024]{1,0:T(1,128)S(1)}, f32[1,1024]{1,0:T(1,128)}, u32[]{:S(2)}) copy-start(f32[1,1024]{1,0:T(1,128)} %get-tuple-element.16) | copy-start | bytes 12292
  95.6 2.2 %copy-start.3 = (f32[1,1024]{1,0:T(1,128)S(1)}, f32[1,1024]{1,0:T(1,128)}, u32[]{:S(2)}) copy-start(f32[1,1024]{1,0:T(1,128)} %get-tuple-element.17) | copy-start | bytes 12292

commit v2 on v1

--- a/solution.py
+++ b/solution.py
@@ -395,7 +395,7 @@
     ug_ref, gg_ref, wg_ref, tap_ref, bias_ref, norm_ref,
     wfull, cotf, lhs_t, hidden, act, gfac, upf, cg, pf32,
     ysend, yrecv, sz1, rz1, sz2, rz2, sf, rf,
-    st, nb, halo_up, halo_cg, up_ref, gate_ref, cw_ref, cb_ref,
+    sy, st, nb, halo_up, halo_cg, cw_ref, cb_ref,
     local_sem, ag_send, ag_recv, yw_send, yw_recv, yp_sem, c_send, c_recv, ry_send, ry_recv,
     rs_send, rs_recv, f_sem, st_recv, st_send, nb_recv, nb_send, hu_sem, hc_sem,
 ):
@@ -410,7 +410,6 @@
     mx, mc = tp // 2, tp % 2
     mate = mx * 2 + (1 - mc)
     mirror = (1 - mx) * 2 + mc
-    across = (1 - mx) * 2 + (1 - mc)
     ynb = mz * y_n + (1 - my)
     sign = (1, -1)
     avail = (mz, z_n - 1 - mz)
@@ -437,8 +436,31 @@
     def drows(zp, y):
         return pl.ds(pl.multiple_of((zp * y_n + y) * dblk, dblk), dblk)
 
+    half_rows = rows // 2
+
     def ccols(owner):
         return cotf.at[:, pl.ds(pl.multiple_of(owner * cshard, cshard), cshard)]
+
+    def chalf(owner, half):
+        tokens = pl.ds(pl.multiple_of(half * half_rows, half_rows), half_rows)
+        return cotf.at[tokens, pl.ds(pl.multiple_of(owner * cshard, cshard), cshard)]
+
+    def urgent(side):
+        outer = side * (z_n - 1)
+        return jnp.where(mz == outer, side * (z_n // 2) + 1 - side, outer)
+
+    def other(side, quarter):
+        return 2 * side * (z_n // 2) + 1 - quarter
+
+    def cx_copy(order, src=None):
+        quarter = urgent(mx) if order == 0 else other(mx, urgent(mx))
+        ref = chalf(quarter, mc)
+        return rcopy(ref if src is None else src, ref, c_send.at[order], c_recv.at[order], me, mirror)
+
+    def cm_copy(order, half):
+        quarter = urgent(1 - mx) if order == 0 else other(1 - mx, urgent(1 - mx))
+        ref = chalf(quarter, half)
+        return rcopy(ref, ref, c_send.at[2 + order], c_recv.at[2 + order], me, mate)
 
     part1, part2 = pl.ds(0, n1), pl.ds(n1, n2)
 
@@ -460,7 +482,8 @@
 
     def rs_copy(d, slot, part, t):
         i = (d * z_n + slot) * 2 + part
-        src, dst = (sz2.at[t], rz2.at[d, t]) if part == 0 else (sz1.at[t], rz1.at[d, t])
+        slot_to = z_n if d == 1 and slot == z_n - 1 else t
+        src, dst = (sz2.at[t], rz2.at[slot_to]) if part == 0 else (sz1.at[t], rz1.at[slot_to])
         return rcopy(src, dst, rs_send.at[i], rs_recv.at[i], nxt[d], tp)
 
     def ry_copy(t):
@@ -471,7 +494,7 @@
     loads = [
         pltpu.make_async_copy(src, dst, local_sem.at[k])
         for k, (src, dst) in enumerate(
-            [(up_hbm, up_ref), (gate_hbm, gate_ref), (cw_hbm, cw_ref), (cb_hbm, cb_ref)], 2
+            [(up_hbm, ug_ref), (gate_hbm, gg_ref), (cw_hbm, cw_ref), (cb_hbm, cb_ref)], 2
         )
     ]
 
@@ -497,8 +520,13 @@
         for d in (0, 1):
             start(functools.partial(ag_copy, d, 0, part, mz), has_next[d])
     start(functools.partial(yw_copy, mz, True))
-    start(lambda: rcopy(cot_hbm, ccols(tp), c_send.at[0], c_recv.at[tp], me, mirror))
-    start(lambda: rcopy(cot_hbm, ccols(tp), c_send.at[1], c_recv.at[tp], me, mate))
+    start(lambda: rcopy(cot_hbm, ccols(tp), c_send.at[4], c_recv.at[4], me, mate))
+    own_half = cot_hbm.at[pl.ds(pl.multiple_of(mc * half_rows, half_rows), half_rows)]
+    leads = urgent(mx) == tp
+
+    @pl.when(leads)
+    def _():
+        cx_copy(0, own_half).start()
 
     for copy in loads:
         copy.wait()
@@ -512,7 +540,21 @@
     def _():
         upf[0:8] = jnp.zeros((8, cols), F32)
 
-    upf[8 : rows + 8] = up_ref[...].astype(F32)
+    rcopy(cot_hbm, ccols(mate), c_send.at[4], c_recv.at[4], me, mate).wait_recv()
+
+    @pl.when(leads)
+    def _():
+        cx_copy(1).start()
+
+    @pl.when(jnp.logical_not(leads))
+    def _():
+        cx_copy(0).start()
+        cx_copy(1, own_half).start()
+
+    sends.append((None, functools.partial(cx_copy, 0)))
+    sends.append((None, functools.partial(cx_copy, 1)))
+
+    upf[8 : rows + 8] = ug_ref[...].astype(F32)
     step = 64
 
     @pl.loop(0, cols // 128)
@@ -526,7 +568,7 @@
             conv = conv + taps[2] * upf[r + 8 : r + 8 + step, lanes]
             sig = 1.0 / (1.0 + jnp.exp(-conv))
             a = conv * sig
-            g = gate_ref[r : r + step, lanes].astype(F32)
+            g = gg_ref[r : r + step, lanes].astype(F32)
             act[r : r + step, lanes] = a
             hidden[r : r + step, lanes] = (a * g).astype(BF16)
             gfac[r : r + step, lanes] = g * sig * (1.0 + conv * (1.0 - sig))
@@ -553,26 +595,28 @@
             lanes = pl.ds(pl.multiple_of(j * 128, 128), 128)
             ysend[t, :, lanes] = pf32[drows(t, 1 - my), lanes].astype(BF16)
 
-    def wg_half(half):
-        low = half * (z_n // 2)
-        first = jnp.where(half == 0, jnp.where(mz == 0, 1, 0), jnp.where(mz == z_n - 1, 0, 1))
-        wg_part(low + first)
-        wg_part(low + 1 - first)
-
-    def ry_start(delta, half=None):
+    def ry_start(delta, only=None):
         for s in sign if delta else (1,):
             t = mz + s * delta
             pred = (t >= 0) & (t < z_n)
             t = (t + z_n) % z_n
-            if half is not None:
-                pred = pred & (t // (z_n // 2) == half)
+            if only is not None:
+                pred = pred & (t == only)
             start(functools.partial(ry_copy, t), pred)
 
+    def wg_far(order):
+        cx = urgent(1 - mx) if order == 0 else other(1 - mx, urgent(1 - mx))
+        rcopy(chalf(cx, mc), chalf(cx, mc), c_send.at[order], c_recv.at[order], me, mirror).wait_recv()
+        start(functools.partial(cm_copy, order, mc))
+        cm_copy(order, 1 - mc).wait_recv()
+        wg_part(cx)
+
     own_c.wait()
-    rcopy(cot_hbm, ccols(mate), c_send.at[1], c_recv.at[mate], me, mate).wait_recv()
-    wg_half(mx)
-    ry_start(z_n - 1, mx)
-
+    wg_part(urgent(mx))
+    ry_start(z_n - 1, urgent(mx))
+    wg_far(0)
+    ry_start(z_n - 1, urgent(1 - mx))
+    wg_part(other(mx, urgent(mx)))
     def ag_step(k):
         for d in (0, 1):
             zp = (mz + z_n - sign[d] * (1 + k)) % z_n
@@ -595,44 +639,35 @@
                     sends.append((fwd, functools.partial(ag_copy, d, k + 1, part, zp)))
             sends.append((is_ag, functools.partial(yw_copy, zp)))
 
-    def rs_step(k):
+    def rs_step(k, part):
         for d in (0, 1):
             t = (mz + z_n - sign[d] * (1 + k)) % z_n
             pred = k >= avail[d]
 
             def run(arrived, d=d, t=t):
+                if part == 1:
+                    ry_copy(t).wait_recv()
                 if arrived:
-                    rs_copy(d, k, 0, t).wait_recv()
-
-                @pl.loop(0, n2 // 128)
+                    rs_copy(d, k, part, t).wait_recv()
+
+                @pl.loop(0, (n1 if part else n2) // 128)
                 def _(j):
-                    far = pl.ds(pl.multiple_of(n1 + j * 128, 128), 128)
                     near = pl.ds(pl.multiple_of(j * 128, 128), 128)
-                    total = pf32[pl.ds(pl.multiple_of(t * ywide, ywide), ywide), far]
+                    if part == 1:
+                        total = pf32[drows(t, my), near] + yrecv[t, :, near].astype(F32)
+                    else:
+                        far = pl.ds(pl.multiple_of(n1 + j * 128, 128), 128)
+                        total = pf32[pl.ds(pl.multiple_of(t * ywide, ywide), ywide), far]
                     if arrived:
-                        total = total + rz2[d, t, :, near].astype(F32)
-                    sz2[t, :, near] = total.astype(BF16)
-
-                rs_copy(d, k + 1, 0, t).start()
-                ry_copy(t).wait_recv()
-                if arrived:
-                    rs_copy(d, k, 1, t).wait_recv()
-
-                @pl.loop(0, n1 // 128)
-                def _(j):
-                    lanes = pl.ds(pl.multiple_of(j * 128, 128), 128)
-                    total = pf32[drows(t, my), lanes] + yrecv[t, :, lanes].astype(F32)
-                    if arrived:
-                        total = total + rz1[d, t, :, lanes].astype(F32)
-                    sz1[t, :, lanes] = total.astype(BF16)
-
-                rs_copy(d, k + 1, 1, t).start()
+                        total = total + (rz1 if part else rz2)[t, :, near].astype(F32)
+                    (sz1 if part else sz2)[t, :, near] = total.astype(BF16)
+
+                rs_copy(d, k + 1, part, t).start()
 
             if k > 0:
                 pl.when(pred & has_prev[d])(functools.partial(run, True))
             pl.when(pred & jnp.logical_not(has_prev[d]))(functools.partial(run, False))
-            for part in (0, 1):
-                sends.append((pred, functools.partial(rs_copy, d, k + 1, part, t)))
+            sends.append((pred, functools.partial(rs_copy, d, k + 1, part, t)))
 
     part_rows = rows // 2 if rows % 32 == 0 else rows
 
@@ -662,25 +697,24 @@
                 hg_add(near, False)
 
     ag_step(0)
-    rcopy(cot_hbm, ccols(mirror), c_send.at[0], c_recv.at[mirror], me, mirror).wait_recv()
-    start(lambda: rcopy(ccols(mirror), ccols(mirror), c_send.at[2], c_recv.at[mirror], me, mate))
-    rcopy(cot_hbm, ccols(across), c_send.at[2], c_recv.at[across], me, mate).wait_recv()
-    wg_half(1 - mx)
-    ry_start(z_n - 1, 1 - mx)
+    rs_step(0, 0)
+    wg_far(1)
     for delta in range(z_n - 2, 1, -1):
         ry_start(delta)
-    rs_step(0)
     own_w.wait()
     yw_wait(mz)
     hg_add(mz, True)
-    for k in range(1, z_n - 1):
-        ag_step(k)
-        if k == 1:
-            ry_start(1)
-        if k == z_n - 2:
-            ry_start(0)
-        rs_step(k)
-        hg_far(k)
+    rs_step(0, 1)
+    ag_step(1)
+    ry_start(1)
+    rs_step(1, 0)
+    rs_step(1, 1)
+    hg_far(1)
+    ag_step(2)
+    ry_start(0)
+    rs_step(2, 0)
+    rs_step(2, 1)
+    hg_far(2)
     hg_far(z_n - 1)
 
     @pl.loop(0, cols // 128)
@@ -706,12 +740,9 @@
             terms = [grad * upf[r + 6 + k : r + 6 + k + step, lanes] for k in range(3)] + [grad]
             sums = [s + jnp.sum(t.reshape(step // 8, 8, 128), axis=0) for s, t in zip(sums, terms)]
         for k in range(4):
-            st[me, k : k + 1, lanes] = jnp.sum(sums[k], axis=0, keepdims=True)
-
-    for d in range(1, fs_n):
-        start(
-            lambda d=d: rcopy(st.at[me], st.at[me], st_send.at[d], st_recv.at[me], (me + d) % fs_n, tp)
-        )
+            sy[my, k : k + 1, lanes] = jnp.sum(sums[k], axis=0, keepdims=True)
+
+    start(lambda: rcopy(sy.at[my], sy.at[my], st_send.at[0], st_recv.at[z_n], ynb, tp))
 
     last = z_n - 1
     for d in (0, 1):
@@ -725,7 +756,7 @@
                 far = pl.ds(pl.multiple_of(n1 + j * 128, 128), 128)
                 near = pl.ds(pl.multiple_of(j * 128, 128), 128)
                 block = pl.ds(pl.multiple_of(mz * ywide, ywide), ywide)
-                pf32[block, far] = pf32[block, far] + rz2[d, mz, :, near].astype(F32)
+                pf32[block, far] = pf32[block, far] + rz2[z_n if d == 1 else mz, :, near].astype(F32)
 
     @pl.loop(0, n2 // 128)
     def _(j):
@@ -735,6 +766,53 @@
 
     f_copy = lambda: rcopy(sf, rf, f_sem.at[0], f_sem.at[1], ynb, tp)
     start(f_copy)
+
+    rcopy(sy.at[1 - my], sy.at[1 - my], st_send.at[0], st_recv.at[z_n], ynb, tp).wait_recv()
+    st[mz] = sy[0] + sy[1]
+    for d in range(1, z_n):
+        start(
+            lambda d=d: rcopy(
+                st.at[mz], st.at[mz], st_send.at[d], st_recv.at[mz], ((mz + d) % z_n) * y_n + my, tp
+            )
+        )
+
+    own_block = drows(mz, my)
+    ry_copy(mz).wait_recv()
+
+    @pl.loop(0, n1 // 128)
+    def _(j):
+        lanes = pl.ds(pl.multiple_of(j * 128, 128), 128)
+        wg_ref[:, lanes] = pf32[own_block, lanes] + yrecv[mz, :, lanes].astype(F32)
+
+    for d in (0, 1):
+
+        @pl.when(has_prev[d])
+        def _():
+            rs_copy(d, last, 1, mz).wait_recv()
+
+            @pl.loop(0, n1 // 128)
+            def _(j):
+                lanes = pl.ds(pl.multiple_of(j * 128, 128), 128)
+                wg_ref[:, lanes] = wg_ref[:, lanes] + rz1[z_n if d == 1 else mz, :, lanes].astype(F32)
+
+    f_copy().wait_recv()
+
+    @pl.loop(0, n2 // 128)
+    def _(j):
+        far = pl.ds(pl.multiple_of(n1 + j * 128, 128), 128)
+        near = pl.ds(pl.multiple_of(j * 128, 128), 128)
+        wg_ref[:, far] = pf32[own_block, far] + rf[:, near].astype(F32)
+
+    @pl.loop(0, cols // 128)
+    def _(j):
+        lanes = pl.ds(pl.multiple_of(j * 128, 128), 128)
+        total = wg_ref[:, lanes]
+        nb[me, :, lanes] = jnp.sum(total * total, axis=0, keepdims=True)
+
+    for d in range(1, fs_n):
+        start(
+            lambda d=d: rcopy(nb.at[me], nb.at[me], nb_send.at[d], nb_recv.at[me], (me + d) % fs_n, tp)
+        )
 
     @pl.when(me < fs_n - 1)
     def _():
@@ -755,50 +833,12 @@
             total = total + taps[2] * cg[r : r + step, lanes]
             ug_ref[r : r + step, lanes] = total.astype(BF16)
 
-    own_block = drows(mz, my)
-    ry_copy(mz).wait_recv()
-
-    @pl.loop(0, n1 // 128)
-    def _(j):
-        lanes = pl.ds(pl.multiple_of(j * 128, 128), 128)
-        wg_ref[:, lanes] = pf32[own_block, lanes] + yrecv[mz, :, lanes].astype(F32)
-
-    for d in (0, 1):
-
-        @pl.when(has_prev[d])
-        def _():
-            rs_copy(d, last, 1, mz).wait_recv()
-
-            @pl.loop(0, n1 // 128)
-            def _(j):
-                lanes = pl.ds(pl.multiple_of(j * 128, 128), 128)
-                wg_ref[:, lanes] = wg_ref[:, lanes] + rz1[d, mz, :, lanes].astype(F32)
-
-    f_copy().wait_recv()
-
-    @pl.loop(0, n2 // 128)
-    def _(j):
-        far = pl.ds(pl.multiple_of(n1 + j * 128, 128), 128)
-        near = pl.ds(pl.multiple_of(j * 128, 128), 128)
-        wg_ref[:, far] = pf32[own_block, far] + rf[:, near].astype(F32)
-
-    @pl.loop(0, cols // 128)
-    def _(j):
-        lanes = pl.ds(pl.multiple_of(j * 128, 128), 128)
-        total = wg_ref[:, lanes]
-        nb[me, :, lanes] = jnp.sum(total * total, axis=0, keepdims=True)
-
-    for d in range(1, fs_n):
-        start(
-            lambda d=d: rcopy(nb.at[me], nb.at[me], nb_send.at[d], nb_recv.at[me], (me + d) % fs_n, tp)
-        )
-
-    for d in range(1, fs_n):
-        owner = (me + d) % fs_n
-        rcopy(st.at[owner], st.at[owner], st_send.at[d], st_recv.at[owner], owner, tp).wait_recv()
+    for d in range(1, z_n):
+        zp = (mz + d) % z_n
+        rcopy(st.at[zp], st.at[zp], st_send.at[d], st_recv.at[zp], zp * y_n + my, tp).wait_recv()
     stats = st[0]
-    for k in range(1, fs_n):
-        stats = stats + st[k]
+    for d in range(1, z_n):
+        stats = stats + st[d]
     tap_ref[...] = stats[0:3]
     bias_ref[...] = stats[3:4]
 
@@ -855,28 +895,27 @@
             pltpu.VMEM((z_n, dblk, n1), BF16),
             pltpu.VMEM((z_n, dblk, n1), BF16),
             pltpu.VMEM((z_n, dblk, n1), BF16),
-            pltpu.VMEM((2, z_n, dblk, n1), BF16),
+            pltpu.VMEM((z_n + 1, dblk, n1), BF16),
             pltpu.VMEM((z_n, ywide, n2), BF16),
-            pltpu.VMEM((2, z_n, ywide, n2), BF16),
+            pltpu.VMEM((z_n + 1, ywide, n2), BF16),
             pltpu.VMEM((dblk, n2), BF16),
             pltpu.VMEM((dblk, n2), BF16),
-            pltpu.VMEM((fs_n, 4, cols), F32),
+            pltpu.VMEM((y_n, 4, cols), F32),
+            pltpu.VMEM((z_n, 4, cols), F32),
             pltpu.VMEM((fs_n, 1, cols), F32),
             pltpu.VMEM((16, cols), BF16),
             pltpu.VMEM((8, cols), F32),
-            pltpu.VMEM((rows, cols), BF16),
-            pltpu.VMEM((rows, cols), BF16),
             pltpu.VMEM((3, cols), F32),
             pltpu.VMEM((1, cols), F32),
             dma((6,)),
             dma((6 * z_n,)), dma((6 * z_n,)), dma((z_n,)), dma((z_n,)), dma((2,)),
-            dma((3,)), dma((tp_n,)), dma((z_n,)), dma((z_n,)),
+            dma((5,)), dma((5,)), dma((z_n,)), dma((z_n,)),
             dma((4 * z_n,)), dma((4 * z_n,)), dma((2,)),
-            dma((fs_n,)), dma((fs_n,)), dma((fs_n,)), dma((fs_n,)),
+            dma((fs_n,)), dma((z_n,)), dma((fs_n,)), dma((fs_n,)),
             dma((2,)), dma((2,)),
         ],
         compiler_params=pltpu.CompilerParams(
-            collective_id=0, has_side_effects=True, vmem_limit_bytes=56000 * 1024
+            collective_id=0, has_side_effects=True, vmem_limit_bytes=46000 * 1024
         ),
     )(*args)
 

time: 98.8 us -> 91.4 us (0.925)
  Pallas kernels: 90.4 us -> 85.6 us
  local copies, waits for them, and re-layouts: 7.36 us -> 5.05 us
    pallas_call x1, Pallas kernels: 90.4 us -> 85.6 us  [line_call(): pl.pallas_call(functools.partial(line_kernel, fs_n, tp_n, y_n, n1), out_s...]
    unnamed x16 -> x6, local copies, waits for them, and re-layouts: 7.36 us -> 5.05 us
where the time goes in v2:
time: 91.4 us; the launch traced here: 91.3 us
  Pallas kernels  85.6 us (94%)
  local copies, waits for them, and re-layouts  5.05 us (6%)
    pallas_call x1, Pallas kernels, line_call(): pl.pallas_call(functools.partial(line_kernel, fs_n, tp_n, y_n, n1), out_s...  85.6 us
    unnamed x6, local copies, waits for them, and re-layouts  5.05 us

profile of v2, /device:TPU:0, one launch (start us, length us, event | category | flops | bytes accessed | tf_op | source)
XLA Modules:
  0.0 91.3 jit_solution(1425075390811193950)
XLA Ops:
  0.6 85.6 %shard_map.109 = (bf16[768,1024]{1,0:T(8,128)(2,1)S(1)}, bf16[768,1024]{1,0:T(8,128)(2,1)S(1)}, f32[256,1024]{1,0:T(8,128)S(1)}, f32[3,1024]{1,0:T(4,128)S(1)}, ...) custom-call(bf16[768,1024]{1,0:T(8,128)(2,1)} %up_hbm.1, bf16[768,1024]{1,0:T(8,128)(2,1)} %gate_hbm.1, ...), custom_call_target="tpu_custom_call" | custom-call | tf_op jit(solution)/shard_map/pallas_call | solution.py:873
  86.2 1.1 %copy.18 = bf16[768,1024]{1,0:T(8,128)(2,1)} copy(bf16[768,1024]{1,0:T(8,128)(2,1)S(1)} %get-tuple-element.24) | data formatting | bytes 3145728
  87.4 1.1 %copy.19 = bf16[768,1024]{1,0:T(8,128)(2,1)} copy(bf16[768,1024]{1,0:T(8,128)(2,1)S(1)} %get-tuple-element.25) | data formatting | bytes 3145728
  88.5 1.0 %copy.20 = f32[256,1024]{1,0:T(8,128)} copy(f32[256,1024]{1,0:T(8,128)S(1)} %get-tuple-element.26) | data formatting | bytes 2097152
  89.5 0.6 copy.21
  90.1 0.6 copy.22
  90.7 0.6 copy.23

commit v3 on v2

--- a/solution.py
+++ b/solution.py
@@ -528,9 +528,45 @@
     def _():
         cx_copy(0, own_half).start()
 
+    rcopy(cot_hbm, ccols(mate), c_send.at[4], c_recv.at[4], me, mate).wait_recv()
+
+    @pl.when(leads)
+    def _():
+        cx_copy(1).start()
+
+    @pl.when(jnp.logical_not(leads))
+    def _():
+        cx_copy(0).start()
+        cx_copy(1, own_half).start()
+
+    sends.append((None, functools.partial(cx_copy, 0)))
+    sends.append((None, functools.partial(cx_copy, 1)))
+
     for copy in loads:
         copy.wait()
 
+    upf[8 : rows + 8] = ug_ref[...].astype(F32)
+    step = 64
+
+    def conv_rows(first, end):
+        @pl.loop(0, cols // 128)
+        def _(j):
+            lanes = pl.ds(pl.multiple_of(j * 128, 128), 128)
+            taps = [cw_ref[k : k + 1, lanes] for k in range(3)]
+            bias = cb_ref[0:1, lanes]
+            for r in range(first, end, step):
+                conv = bias + taps[0] * upf[r + 6 : r + 6 + step, lanes]
+                conv = conv + taps[1] * upf[r + 7 : r + 7 + step, lanes]
+                conv = conv + taps[2] * upf[r + 8 : r + 8 + step, lanes]
+                sig = 1.0 / (1.0 + jnp.exp(-conv))
+                a = conv * sig
+                g = gg_ref[r : r + step, lanes].astype(F32)
+                act[r : r + step, lanes] = a
+                hidden[r : r + step, lanes] = (a * g).astype(BF16)
+                gfac[r : r + step, lanes] = g * sig * (1.0 + conv * (1.0 - sig))
+
+    conv_rows(step, rows)
+
     @pl.when(me > 0)
     def _():
         rcopy(halo_up, halo_up, hu_sem.at[0], hu_sem.at[1], (me + fs_n - 1) % fs_n, tp).wait_recv()
@@ -540,38 +576,7 @@
     def _():
         upf[0:8] = jnp.zeros((8, cols), F32)
 
-    rcopy(cot_hbm, ccols(mate), c_send.at[4], c_recv.at[4], me, mate).wait_recv()
-
-    @pl.when(leads)
-    def _():
-        cx_copy(1).start()
-
-    @pl.when(jnp.logical_not(leads))
-    def _():
-        cx_copy(0).start()
-        cx_copy(1, own_half).start()
-
-    sends.append((None, functools.partial(cx_copy, 0)))
-    sends.append((None, functools.partial(cx_copy, 1)))
-
-    upf[8 : rows + 8] = ug_ref[...].astype(F32)
-    step = 64
-
-    @pl.loop(0, cols // 128)
-    def _(j):
-        lanes = pl.ds(pl.multiple_of(j * 128, 128), 128)
-        taps = [cw_ref[k : k + 1, lanes] for k in range(3)]
-        bias = cb_ref[0:1, lanes]
-        for r in range(0, rows, step):
-            conv = bias + taps[0] * upf[r + 6 : r + 6 + step, lanes]
-            conv = conv + taps[1] * upf[r + 7 : r + 7 + step, lanes]
-            conv = conv + taps[2] * upf[r + 8 : r + 8 + step, lanes]
-            sig = 1.0 / (1.0 + jnp.exp(-conv))
-            a = conv * sig
-            g = gg_ref[r : r + step, lanes].astype(F32)
-            act[r : r + step, lanes] = a
-            hidden[r : r + step, lanes] = (a * g).astype(BF16)
-            gfac[r : r + step, lanes] = g * sig * (1.0 + conv * (1.0 - sig))
+    conv_rows(0, step)
 
     rcopy(
         w_hbm.at[:, part2], wfull.at[drows(mz, 1 - my), part2], yp_sem.at[0], yp_sem.at[1], ynb, tp
@@ -595,49 +600,44 @@
             lanes = pl.ds(pl.multiple_of(j * 128, 128), 128)
             ysend[t, :, lanes] = pf32[drows(t, 1 - my), lanes].astype(BF16)
 
-    def ry_start(delta, only=None):
-        for s in sign if delta else (1,):
-            t = mz + s * delta
-            pred = (t >= 0) & (t < z_n)
-            t = (t + z_n) % z_n
-            if only is not None:
-                pred = pred & (t == only)
-            start(functools.partial(ry_copy, t), pred)
+    first, second = urgent(mx), urgent(1 - mx)
+    third, fourth = other(mx, first), other(1 - mx, second)
+
+    def ry_start(t, delta=None):
+        pred = None if delta is None else jnp.abs(t - mz) == delta
+        start(functools.partial(ry_copy, t), pred)
 
     def wg_far(order):
-        cx = urgent(1 - mx) if order == 0 else other(1 - mx, urgent(1 - mx))
+        cx = fourth if order else second
         rcopy(chalf(cx, mc), chalf(cx, mc), c_send.at[order], c_recv.at[order], me, mirror).wait_recv()
         start(functools.partial(cm_copy, order, mc))
         cm_copy(order, 1 - mc).wait_recv()
         wg_part(cx)
 
     own_c.wait()
-    wg_part(urgent(mx))
-    ry_start(z_n - 1, urgent(mx))
+    wg_part(first)
+    ry_start(first)
     wg_far(0)
-    ry_start(z_n - 1, urgent(1 - mx))
-    wg_part(other(mx, urgent(mx)))
-    def ag_step(k):
+    ry_start(second, z_n - 1)
+    def ag_step(k, part):
         for d in (0, 1):
             zp = (mz + z_n - sign[d] * (1 + k)) % z_n
             is_ag = k < avail[d]
-            fwd = is_ag & has_next[d]
 
             @pl.when(is_ag)
             def _():
-                for part in (0, 1, 2):
-                    ag_copy(d, k, part, zp).wait_recv()
-                    if k + 1 < z_n - 1:
-                        @pl.when(has_next[d])
-                        def _():
-                            ag_copy(d, k + 1, part, zp).start()
-                    if part == 1:
-                        yw_copy(zp).start()
-
-            for part in (0, 1, 2):
+                ag_copy(d, k, part, zp).wait_recv()
                 if k + 1 < z_n - 1:
-                    sends.append((fwd, functools.partial(ag_copy, d, k + 1, part, zp)))
-            sends.append((is_ag, functools.partial(yw_copy, zp)))
+                    @pl.when(has_next[d])
+                    def _():
+                        ag_copy(d, k + 1, part, zp).start()
+                if part == 1:
+                    yw_copy(zp).start()
+
+            if k + 1 < z_n - 1:
+                sends.append((is_ag & has_next[d], functools.partial(ag_copy, d, k + 1, part, zp)))
+            if part == 1:
+                sends.append((is_ag, functools.partial(yw_copy, zp)))
 
     def rs_step(k, part):
         for d in (0, 1):
@@ -696,23 +696,36 @@
                 yw_wait(near)
                 hg_add(near, False)
 
-    ag_step(0)
+    ag_step(0, 0)
+    ag_step(0, 1)
+    for delta in range(z_n - 2, 1, -1):
+        ry_start(second, delta)
     rs_step(0, 0)
+    wg_part(third)
+    for delta in range(z_n - 2, 1, -1):
+        ry_start(third, delta)
+    ag_step(0, 2)
     wg_far(1)
     for delta in range(z_n - 2, 1, -1):
-        ry_start(delta)
+        ry_start(fourth, delta)
     own_w.wait()
     yw_wait(mz)
     hg_add(mz, True)
     rs_step(0, 1)
-    ag_step(1)
-    ry_start(1)
+    ag_step(1, 0)
+    ag_step(1, 1)
+    for t in (second, third, fourth):
+        ry_start(t, 1)
     rs_step(1, 0)
+    ag_step(1, 2)
     rs_step(1, 1)
     hg_far(1)
-    ag_step(2)
-    ry_start(0)
+    ag_step(2, 0)
+    ag_step(2, 1)
+    for t in (second, third, fourth):
+        ry_start(t, 0)
     rs_step(2, 0)
+    ag_step(2, 2)
     rs_step(2, 1)
     hg_far(2)
     hg_far(z_n - 1)

time: 91.4 us -> 84.8 us (0.928)
  Pallas kernels: 85.6 us -> 79 us
    pallas_call x1, Pallas kernels: 85.6 us -> 79 us  [line_call(): pl.pallas_call(functools.partial(line_kernel, fs_n, tp_n, y_n, n1), out_s...]
where the time goes in v3:
time: 84.8 us; the launch traced here: 84.7 us
  Pallas kernels  79 us (93%)
  local copies, waits for them, and re-layouts  5.05 us (6%)
    pallas_call x1, Pallas kernels, line_call(): pl.pallas_call(functools.partial(line_kernel, fs_n, tp_n, y_n, n1), out_s...  79 us
    unnamed x6, local copies, waits for them, and re-layouts  5.05 us

profile of v3, /device:TPU:0, one launch (start us, length us, event | category | flops | bytes accessed | tf_op | source)
XLA Modules:
  0.0 84.7 jit_solution(12317314227183052813)
XLA Ops:
  0.6 79.0 %shard_map.109 = (bf16[768,1024]{1,0:T(8,128)(2,1)S(1)}, bf16[768,1024]{1,0:T(8,128)(2,1)S(1)}, f32[256,1024]{1,0:T(8,128)S(1)}, f32[3,1024]{1,0:T(4,128)S(1)}, ...) custom-call(bf16[768,1024]{1,0:T(8,128)(2,1)} %up_hbm.1, bf16[768,1024]{1,0:T(8,128)(2,1)} %gate_hbm.1, ...), custom_call_target="tpu_custom_call" | custom-call | tf_op jit(solution)/shard_map/pallas_call | solution.py:886
  79.6 1.1 %copy.18 = bf16[768,1024]{1,0:T(8,128)(2,1)} copy(bf16[768,1024]{1,0:T(8,128)(2,1)S(1)} %get-tuple-element.24) | data formatting | bytes 3145728
  80.8 1.1 %copy.19 = bf16[768,1024]{1,0:T(8,128)(2,1)} copy(bf16[768,1024]{1,0:T(8,128)(2,1)S(1)} %get-tuple-element.25) | data formatting | bytes 3145728
  81.9 1.0 %copy.20 = f32[256,1024]{1,0:T(8,128)} copy(f32[256,1024]{1,0:T(8,128)S(1)} %get-tuple-element.26) | data formatting | bytes 2097152
  82.9 0.6 copy.21
  83.5 0.6 copy.22
  84.1 0.6 copy.23

commit v4 on v3

--- a/solution.py
+++ b/solution.py
@@ -933,6 +933,27 @@
     )(*args)
 
 
+def write_kernel(*refs):
+    count = len(refs) // 2
+    sem = refs[-1]
+    copies = [pltpu.make_async_copy(refs[k], refs[count + k], sem.at[k]) for k in range(count)]
+    for copy in copies:
+        copy.start()
+    for copy in copies:
+        copy.wait()
+
+
+def write_out(values):
+    return pl.pallas_call(
+        write_kernel,
+        out_shape=tuple(jax.ShapeDtypeStruct(v.shape, v.dtype) for v in values),
+        in_specs=[pl.BlockSpec(memory_space=pltpu.VMEM)] * len(values),
+        out_specs=[pl.BlockSpec(memory_space=pltpu.HBM)] * len(values),
+        scratch_shapes=[pltpu.SemaphoreType.DMA((len(values),))],
+        compiler_params=pltpu.CompilerParams(vmem_limit_bytes=1024 * 1024),
+    )(*values)
+
+
 def per_device(fs_n, tp_n, up_pre, gate_value, out_cotangent, down_weight, conv_weight, conv_bias):
     rows, cols = up_pre.shape
     dblk = down_weight.shape[0]
@@ -944,7 +965,7 @@
         for value in (up_pre, gate_value, out_cotangent, down_weight, conv_weight, conv_bias[None, :])
     )
     if tp_n == 4 and z_n == tp_n and rows % 64 == 0 and cols % 256 == 0 and dblk % 128 == 0:
-        outs = line_call(fs_n, tp_n, y_n, args)
+        outs = write_out(line_call(fs_n, tp_n, y_n, args))
     else:
         outs = general_call(fs_n, tp_n, y_n, args)
     ug, gg, wg, tap, bias, norm = outs

time: 84.8 us -> 81.9 us (0.966)
  local copies, waits for them, and re-layouts: 5.05 us -> 0 us
  Pallas kernels: 79 us -> 81.1 us
    unnamed x6 -> x0, local copies, waits for them, and re-layouts: 5.05 us -> none
    pallas_call x0 -> x1, Pallas kernels: none -> 2.07 us  [write_out(): pl.pallas_call(write_kernel, out_shape=tuple((jax.ShapeDtypeStruct(v.shap...]
where the time goes in v4:
time: 81.9 us; the launch traced here: 81.7 us
  Pallas kernels  81.1 us (99%)
    pallas_call x1, Pallas kernels, line_call(): pl.pallas_call(functools.partial(line_kernel, fs_n, tp_n, y_n, n1), out_s...  79 us
    pallas_call x1, Pallas kernels, write_out(): pl.pallas_call(write_kernel, out_shape=tuple((jax.ShapeDtypeStruct(v.shap...  2.07 us

profile of v4, /device:TPU:0, one launch (start us, length us, event | category | flops | bytes accessed | tf_op | source)
XLA Modules:
  0.0 81.7 jit_solution(9008501747191116289)
XLA Ops:
  0.6 79.0 %shard_map.109 = (bf16[768,1024]{1,0:T(8,128)(2,1)S(1)}, bf16[768,1024]{1,0:T(8,128)(2,1)S(1)}, f32[256,1024]{1,0:T(8,128)S(1)}, f32[3,1024]{1,0:T(4,128)S(1)}, ...) custom-call(bf16[768,1024]{1,0:T(8,128)(2,1)} %up_hbm.1, bf16[768,1024]{1,0:T(8,128)(2,1)} %gate_hbm.1, ...), custom_call_target="tpu_custom_call" | custom-call | tf_op jit(solution)/shard_map/pallas_call | solution.py:886
  79.6 2.1 %shard_map.110 = (bf16[768,1024]{1,0:T(8,128)(2,1)}, bf16[768,1024]{1,0:T(8,128)(2,1)}, f32[256,1024]{1,0:T(8,128)}, f32[3,1024]{1,0:T(4,128)}, f32[1,1024]{1,0:T(1,128)}, /*index=5*/f32[1,1024]{1,0:T(1,128)}) custom-call(bf16[768,1024]{1,0:T(8,128)(2,1)S(1)} %get-tuple-element.18.refs_0_, bf16[768,1024]{1,0:T(8,128)(2,1)S(1)} %get-tuple-element.19.refs_1_, ...), custom_call_target="tpu_custom_call" | custom-call | tf_op jit(solution)/shard_map/pallas_call | solution.py:947
